TPU v7x, 256 devices: a whole 4x4x8 slice. The times are simulated.
256 devices in a mesh: ep: 64 (over z, x, core), tp: 4 (over y).
Axes of the slice: x: 4, y: 4, z: 8, core: 2. Of those that a mesh axis runs over, the one named last changes fastest.
Arguments:
- out_gate: bfloat16 [32768, 2048], P(('ep', 'tp')), may hold values from -6 to 6
- in_gate: bfloat16 [32768, 2048], P(('ep', 'tp')), may hold values from -6 to 6
- conv_input: bfloat16 [32768, 2048], P(('ep', 'tp')), may hold values from -6 to 6
- conv_taps: bfloat16 [3, 2048], replicated, may hold values from -3 to 3
- mixer_weight: bfloat16 [2048, 2048], P(None, 'tp'), may hold values from -0.125 to 0.125
- expert_input: bfloat16 [32768, 2048], P(('ep', 'tp')), may hold values from -6 to 6
- norm_gain: float32 [2048], replicated, may hold values from 0.1 to 1.9
- expert_gate: bfloat16 [64, 2048, 1024], P('ep', None, 'tp'), may hold values from -0.125 to 0.125
- expert_up: bfloat16 [64, 2048, 1024], P('ep', None, 'tp'), may hold values from -0.125 to 0.125
- expert_down: bfloat16 [64, 1024, 2048], P('ep', 'tp'), may hold values from -0.1875 to 0.1875
- expert_ids: int32 [32768, 2], P(('ep', 'tp')), may hold values from 0 to 63, all different within a row; in each aligned block of 128 rows (0 to 127, 128 to 255, ...) at most 8 rows name the same one
- route_weight: float32 [32768, 2], P(('ep', 'tp')), may hold values from 0.1 to 1
Outputs:
- mixer_out: bfloat16 [32768, 2048], P('ep', 'tp')
- experts_out: bfloat16 [32768, 2048], P(('ep', 'tp'))
Inputs may be any that keep to these rules, and one draw needn't show every extreme that they name: `expert_ids`: each row names 2 different experts. Within the 128 rows of one device no expert is named by more than 8 rows, and in some devices' rows some expert is named by exactly 8.
All inputs are finite; a program needn't handle non-finite values.
Results may differ from a plain program's by a relative error of at most 0.011.
Values may be sent and summed in bfloat16 or wider, within the bound.
No kernel may reach another device: no remote copies, remote signals or barrier semaphores. Data moves between devices by JAX's collectives and lax.ppermute only.
A program may use at most 128 MiB of HBM per device.

v0:
```python
import jax
import jax.numpy as jnp
from jax import lax
from jax.sharding import PartitionSpec as P

CONV = 3
SEQS = 1
norm_eps = 1e-06


def from_behind(value, axis, steps):
    count = lax.axis_size(axis)
    first, last = (max(0, -steps), min(count, count - steps))
    return lax.ppermute(value, axis, [(source, source + steps) for source in range(first, last)])


def turned_gather(arrays, axis, dims):
    turned = [jnp.moveaxis(a, dim, 0) for a, dim in zip(arrays, dims)]
    both = jnp.concatenate([t.reshape(len(t), -1) for t in turned], axis=1)
    whole, at, done = (lax.all_gather(both, axis, axis=0, tiled=True), 0, [])
    for t, dim in zip(turned, dims):
        piece = whole[:, at : at + t[0].size].reshape(-1, *t.shape[1:])
        done.append(jnp.moveaxis(piece, 0, dim))
        at += t[0].size
    return tuple(done)


def sent_to_all(x, axis):
    count = lax.axis_size(axis)
    return lax.all_to_all(jnp.broadcast_to(x[None], (count, *x.shape)), axis, 0, 0, tiled=True)


def joined_along(tiles, dim):
    dims = list(tiles.shape[1:])
    dims[dim] *= tiles.shape[0]
    return jnp.moveaxis(tiles, 0, dim).reshape(dims)


def gathered_copies(x, axis, dim):
    tiles = sent_to_all(x, axis)
    return joined_along(tiles, dim)


def device_slots(route_ids, expert_count):
    flat_ids = route_ids.reshape(-1)
    member = (flat_ids[:, None] == jnp.arange(expert_count, dtype=jnp.int32)[None, :]).astype(
        jnp.int32
    )
    before = jnp.cumsum(member, axis=0) - member
    return jnp.sum(before * member, axis=1).reshape(route_ids.shape)


def fill_slots(row_data, route_ids, expert_count, slot_cap):
    top_count = route_ids.shape[1]
    position = (route_ids * slot_cap + device_slots(route_ids, expert_count)).reshape(-1)
    zeroed = jnp.zeros((expert_count * slot_cap, row_data.shape[1]), row_data.dtype)
    return zeroed.at[position].set(jnp.repeat(row_data, top_count, axis=0))


def expert_hidden(slot_rows, w_gate, w_up):
    gate_proj = jnp.dot(slot_rows, w_gate, preferred_element_type=jnp.float32)
    up_proj = jnp.dot(slot_rows, w_up, preferred_element_type=jnp.float32)
    return (jax.nn.silu(gate_proj) * up_proj).astype(jnp.bfloat16)


def local(
    out_gate,
    in_gate,
    conv_input,
    conv_taps,
    mixer_weight,
    expert_input,
    norm_gain,
    expert_gate,
    expert_up,
    expert_down,
    expert_ids,
    route_weight,
):
    row_count = in_gate.shape[0]
    tap_span = CONV - 1
    group_size = lax.axis_size("tp")
    product = in_gate.astype(jnp.float32) * conv_input.astype(jnp.float32)
    edge_product = from_behind(product[row_count - tap_span :], ("ep", "tp"), 1)
    seq_length = row_count * lax.axis_size("ep") * group_size // SEQS
    linear_index = lax.axis_index("ep") * group_size + lax.axis_index("tp")
    carry_over = jnp.where(linear_index * row_count % seq_length == 0, 0.0, 1.0).astype(jnp.float32)
    earlier = edge_product * carry_over
    padded = jnp.concatenate([earlier, product], axis=0)
    tap_values = conv_taps.astype(jnp.float32)
    smoothed = sum(
        (
            padded[tap_index : tap_index + row_count] * tap_values[tap_index]
            for tap_index in range(CONV)
        )
    )
    gated = (out_gate.astype(jnp.float32) * smoothed).astype(jnp.bfloat16)
    token_count = expert_input.shape[0]
    model_width = expert_input.shape[1]
    expert_count = lax.axis_size("ep")
    slot_cap = 4 * token_count // expert_count
    wide_input = expert_input.astype(jnp.float32)
    inv_norm = lax.rsqrt(jnp.mean(wide_input * wide_input, axis=1, keepdims=True) + norm_eps)
    normed = (wide_input * inv_norm * norm_gain).astype(jnp.bfloat16)
    w_gate = expert_gate[0]
    hidden_width = w_gate.shape[1]
    position = (expert_ids * slot_cap + device_slots(expert_ids, expert_count)).reshape(-1)
    whole_gate, whole_up, whole_down = turned_gather(
        (expert_gate, expert_up, expert_down), "tp", (2, 2, 1)
    )
    mixer_out = jnp.dot(
        gathered_copies(gated, "tp", 0), mixer_weight, preferred_element_type=jnp.float32
    ).astype(jnp.bfloat16)
    outgoing = fill_slots(normed, expert_ids, expert_count, slot_cap).reshape(
        expert_count, slot_cap, model_width
    )
    arrived = lax.all_to_all(outgoing, "ep", split_axis=0, concat_axis=0, tiled=True)
    hidden = expert_hidden(arrived.reshape(-1, model_width), whole_gate[0], whole_up[0])
    running = jnp.zeros((hidden.shape[0], model_width), jnp.float32)
    for quarter in range(group_size):
        partial_sum = jnp.dot(
            hidden[:, quarter * hidden_width : (quarter + 1) * hidden_width],
            whole_down[0, quarter * hidden_width : (quarter + 1) * hidden_width],
            preferred_element_type=jnp.float32,
        )
        running = running + lax.optimization_barrier(partial_sum.astype(jnp.bfloat16)).astype(
            jnp.float32
        )
    summed = running.astype(jnp.bfloat16)
    returned = lax.all_to_all(
        summed.reshape(expert_count, slot_cap, model_width),
        "ep",
        split_axis=0,
        concat_axis=0,
        tiled=True,
    )
    picked = returned.reshape(expert_count * slot_cap, model_width)[position]
    top_count = expert_ids.shape[1]
    picked = picked.reshape(token_count, top_count, model_width).astype(jnp.float32)
    route_share = route_weight / jnp.sum(route_weight, axis=1, keepdims=True)
    experts_out = jnp.sum(picked * route_share[:, :, None], axis=1).astype(jnp.bfloat16)
    return (mixer_out, experts_out)


def solution(mesh):
    return jax.shard_map(
        local,
        mesh=mesh,
        in_specs=(
            P(("ep", "tp"), None),
            P(("ep", "tp"), None),
            P(("ep", "tp"), None),
            P(),
            P(None, "tp"),
            P(("ep", "tp"), None),
            P(),
            P("ep", None, "tp"),
            P("ep", None, "tp"),
            P("ep", "tp", None),
            P(("ep", "tp"), None),
            P(("ep", "tp"), None),
        ),
        out_specs=(P("ep", "tp"), P(("ep", "tp"), None)),
        check_vma=False,
    )
```

profile of v0, /device:TPU:2, one launch (start us, length us, event | category | flops | bytes accessed | tf_op | source)
XLA Modules:
  0.0 256.6 jit_solution(5777766313457616433)
XLA Ops:
  7.2 0.0 copy-start
  7.2 0.0 all-gather.2.cloned.1.call-start
  7.2 1.6 copy.31
  8.9 2.3 copy.30
  11.1 3.0 %pad_maximum_fusion = bf16[256,6144]{1,0:T(8,128)(2,1)} fusion(bf16[256,2048]{1,0:T(8,128)(2,1)} %bitcast.77, bf16[256,2048]{1,0:T(8,128)(2,1)S(1)} %bitcast.75, bf16[256,2048]{1,0:T(8,128)(2,1)} %bitcast.76), kind=kLoop, calls=%fused_computation.8 | loop fusion | flops 9437184 | bytes 6291456 | tf_op jit(solution)/shard_map/concatenate | solution.py:19
  14.2 0.0 all-gather.2.cloned.1.call-update
  14.2 0.6 copy-done.6
  14.8 0.1 copy.25
  14.9 0.1 eq.42
  15.1 0.1 eq.38
  15.2 0.6 reduce-window.6
  15.8 0.2 slice_reduce_fusion
  16.1 0.1 fusion.25
  16.2 0.1 reshape.104
  16.3 0.1 copy.28
  16.4 0.1 copy.29
  16.5 0.1 reshape.105
  16.7 0.2 fusion.13
  16.9 0.2 fusion.15
  17.1 0.6 broadcast_in_dim.8
  17.7 1.2 reshape.128
  19.0 4.4 %scatter_custom_fusion = bf16[512,2048]{1,0:T(8,128)(2,1)} fusion(s32[256]{0:T(256)S(1)} %bitcast.81, bf16[256,2048]{1,0:T(8,128)(2,1)} %reshape.128, bf16[]{:T(256)} %constant.45.clone.1), kind=kCustom, calls=%fused_computation.38 | custom fusion | bytes 2097664 | tf_op jit(solution)/shard_map/scatter | solution.py:57
  23.4 12.2 %all-to-all-start.1 = ((bf16[64,8,2048]{2,1,0:T(8,128)(2,1)}), bf16[64,8,2048]{2,1,0:T(8,128)(2,1)}, u32[]{:S(2)}, u32[]{:S(2)}) async-start(bf16[64,8,2048]{2,1,0:T(8,128)(2,1)} %bitcast.74), calls=%async_computation.1 | async-start | bytes 4194304 | tf_op jit(solution)/shard_map/all_to_all | solution.py:117
  35.6 0.0 copy-start.4
  35.6 1.4 convert_multiply_fusion.2
  37.1 3.5 %collective-permute-start = (f32[2,2048]{1,0:T(2,128)S(1)}, f32[2,2048]{1,0:T(2,128)S(1)}, u32[]{:S(2)}, u32[]{:S(2)}) collective-permute-start(f32[2,2048]{1,0:T(2,128)S(1)} %slice.78), channel_id=1, source_target_pairs={{0,1},{1,2},{2,3},{3,4},{4,5},{5,6},{6,7},{7,8},{8,9},{9,10},{10,1... | collective-permute-start | bytes 49160 | tf_op jit(solution)/shard_map/ppermute | solution.py:14
  40.6 3.7 %collective-permute-done = f32[2,2048]{1,0:T(2,128)S(1)} collective-permute-done((f32[2,2048]{1,0:T(2,128)S(1)}, f32[2,2048]{1,0:T(2,128)S(1)}, u32[]{:S(2)}, u32[]{:S(2)}) %collective-permute-start) | collective-permute-done | bytes 16416 | tf_op jit(solution)/shard_map/ppermute | solution.py:14
  44.4 2.2 fusion.12
  46.6 91.8 %all-gather.2.cloned.1.call-done = bf16[1024,6144]{1,0:T(8,128)(2,1)} async-done(((bf16[256,6144]{1,0:T(8,128)(2,1)}), bf16[1024,6144]{1,0:T(8,128)(2,1)}) %all-gather.2.cloned.1.call-update) | async-done | bytes 12582928 | tf_op jit(solution)/shard_map/all_gather | solution.py:20
  138.4 4.7 %slice_bitcast_fusion = bf16[1,1024,2048]{2,1,0:T(8,128)(2,1)} fusion(bf16[1024,6144]{1,0:T(8,128)(2,1)} %all-gather.2.cloned.1.call-done), kind=kLoop, calls=%fused_computation.2 | loop fusion | bytes 8388608 | tf_op jit(solution)/shard_map/transpose;reshape | solution.py:23
  143.1 0.0 all-to-all-done.1
  143.1 1.6 broadcast_in_dim.6
  144.7 4.6 %all-to-all-start = ((bf16[4,128,2048]{2,1,0:T(8,128)(2,1)}), bf16[4,128,2048]{2,1,0:T(8,128)(2,1)}, u32[]{:S(2)}, u32[]{:S(2)}) async-start(bf16[4,128,2048]{2,1,0:T(8,128)(2,1)} %broadcast_in_dim.6), calls=%async_computation | async-start | bytes 4194304 | tf_op jit(solution)/shard_map/all_to_all | solution.py:30
  149.4 5.2 %fusion.1 = f32[512,1024]{1,0:T(8,128)S(1)} fusion(bf16[1024,6144]{1,0:T(8,128)(2,1)} %all-gather.2.cloned.1.call-done, bf16[64,8,2048]{2,1,0:T(8,128)(2,1)} %all-to-all-done.1), kind=kOutput, calls=%fused_computation.6 | convolution fusion | flops 2147483648 | bytes 8388608 | tf_op jit(solution)/shard_map/dot_general | solution.py:61
  154.6 5.5 %multiply_convert_fusion = bf16[512,1024]{1,0:T(8,128)(2,1)S(1)} fusion(f32[512,1024]{1,0:T(8,128)S(1)} %fusion.1, bf16[1024,6144]{1,0:T(8,128)(2,1)} %all-gather.2.cloned.1.call-done, bf16[64,8,2048]{2,1,0:T(8,128)(2,1)} %all-to-all-done.1), kind=kOutput, calls=%fused_computation.17 | convolution fusion | flops 2150629376 | bytes 9437184 | tf_op jit(solution)/shard_map/dot_general | solution.py:62
  160.1 0.7 convolution_convert_fusion.3
  160.8 0.7 convolution_convert_fusion.2
  161.5 0.7 convolution_convert_fusion.1
  162.2 0.7 convolution_convert_fusion
  163.0 3.1 %fusion.2 = bf16[64,8,2048]{2,1,0:T(8,128)(2,1)} fusion(bf16[512,2048]{1,0:T(8,128)(2,1)S(1)} %convolution_convert_fusion, bf16[512,2048]{1,0:T(8,128)(2,1)S(1)} %convolution_convert_fusion.1, bf16[512,2048]{1,0:T(8,128)(2,1)S(1)} %convolution_convert_fusion.2, bf16[512,2048]{1,0:T(8,128)(2,1)S(1)} %convolution_convert_fusion.3), kind=kLoop, calls=%fused_computation.13 | loop fusion | flops 8388608 | bytes 10485760 | tf_op jit(solution)/shard_map/reshape | solution.py:131
  166.1 9.6 %all-to-all-done = bf16[4,128,2048]{2,1,0:T(8,128)(2,1)} async-done(((bf16[4,128,2048]{2,1,0:T(8,128)(2,1)}), bf16[4,128,2048]{2,1,0:T(8,128)(2,1)}, u32[]{:S(2)}, u32[]{:S(2)}) %all-to-all-start) | async-done | bytes 2097184 | tf_op jit(solution)/shard_map/all_to_all | solution.py:30
  175.7 10.7 %all-to-all-start.2 = ((bf16[64,8,2048]{2,1,0:T(8,128)(2,1)}), bf16[64,8,2048]{2,1,0:T(8,128)(2,1)}, u32[]{:S(2)}, u32[]{:S(2)}) async-start(bf16[64,8,2048]{2,1,0:T(8,128)(2,1)} %fusion.2), calls=%async_computation.2 | async-start | bytes 4194304 | tf_op jit(solution)/shard_map/all_to_all | solution.py:130
  186.5 0.1 copy.32
  186.6 3.6 %convolution_convert_fusion.4 = bf16[512,512]{1,0:T(8,128)(2,1)} fusion(bf16[512,2048]{1,0:T(8,128)(2,1)} %bitcast.3, bf16[2048,512]{1,0:T(8,128)(2,1)S(1)} %copy-done), kind=kOutput, calls=%fused_computation.20 | convolution fusion | flops 1074003968 | bytes 4718592 | tf_op jit(solution)/shard_map/dot_general | solution.py:111
  190.2 47.3 %all-to-all-done.2 = bf16[64,8,2048]{2,1,0:T(8,128)(2,1)} async-done(((bf16[64,8,2048]{2,1,0:T(8,128)(2,1)}), bf16[64,8,2048]{2,1,0:T(8,128)(2,1)}, u32[]{:S(2)}, u32[]{:S(2)}) %all-to-all-start.2) | async-done | bytes 2097184 | tf_op jit(solution)/shard_map/all_to_all | solution.py:130
  237.6 4.2 %gather_fusion = bf16[256,2048]{1,0:T(8,128)(2,1)S(1)} fusion(bf16[512,2048]{1,0:T(8,128)(2,1)} %bitcast.25, s32[1024]{0:T(1024)S(1)} %pad_clamp_fusion), kind=kCustom, calls=%fused_computation | custom fusion | bytes 2098176 | tf_op jit(solution)/shard_map/gather | solution.py:137
  241.8 2.4 reshape.115
  244.2 5.6 %multiply_reduce_fusion = bf16[128,2048]{1,0:T(8,128)(2,1)} fusion(f32[128,2,2048]{2,1,0:T(2,128)} %reshape.115, f32[128,2]{1,0:T(8,128)S(1)} %copy.32), kind=kLoop, calls=%fused_computation.16 | loop fusion | flops 786432 | bytes 2622464 | tf_op jit(solution)/shard_map/reduce_sum | solution.py:141
  (25 shorter events, 0.2 us)
Async XLA Ops:
  7.2 179.4 %copy-start = (bf16[2048,512]{1,0:T(8,128)(2,1)S(1)}, bf16[2048,512]{1,0:T(8,128)(2,1)}, u32[]{:S(2)}) copy-start(bf16[2048,512]{1,0:T(8,128)(2,1)} %param.16) | copy-start | bytes 6291460
  7.2 131.2 %all-gather.2.cloned.1.call-start = ((), (), s32[]{:S(2)}) async-start(), calls=%async_computation.3 | async-start | bytes 15728640 | tf_op jit(solution)/shard_map/all_gather | solution.py:20
  14.1 0.7 copy-start.6
  14.1 2.5 copy-start.2
  14.1 2.7 %copy-start.5 = (f32[2048]{0:T(1024)S(1)}, f32[2048]{0:T(1024)}, u32[]{:S(2)}) copy-start(f32[2048]{0:T(1024)} %param.18) | copy-start | bytes 24580
  23.4 119.7 %all-to-all-start.1 = ((bf16[64,8,2048]{2,1,0:T(8,128)(2,1)}), bf16[64,8,2048]{2,1,0:T(8,128)(2,1)}, u32[]{:S(2)}, u32[]{:S(2)}) async-start(bf16[64,8,2048]{2,1,0:T(8,128)(2,1)} %bitcast.74), calls=%async_computation.1 | async-start | bytes 4194304 | tf_op jit(solution)/shard_map/all_to_all | solution.py:117
  35.6 5.0 %copy-start.4 = (bf16[3,2048]{1,0:T(4,128)(2,1)S(1)}, bf16[3,2048]{1,0:T(4,128)(2,1)}, u32[]{:S(2)}) copy-start(bf16[3,2048]{1,0:T(4,128)(2,1)} %param.15) | copy-start | bytes 36868
  37.1 7.3 %collective-permute-start = (f32[2,2048]{1,0:T(2,128)S(1)}, f32[2,2048]{1,0:T(2,128)S(1)}, u32[]{:S(2)}, u32[]{:S(2)}) collective-permute-start(f32[2,2048]{1,0:T(2,128)S(1)} %slice.78), channel_id=1, source_target_pairs={{0,1},{1,2},{2,3},{3,4},{4,5},{5,6},{6,7},{7,8},{8,9},{9,10},{10,1... | collective-permute-start | bytes 49160 | tf_op jit(solution)/shard_map/ppermute | solution.py:14
  46.6 96.5 %copy-start.3 = (bf16[128,2048]{1,0:T(8,128)(2,1)S(1)}, bf16[128,2048]{1,0:T(8,128)(2,1)}, u32[]{:S(2)}) copy-start(bf16[128,2048]{1,0:T(8,128)(2,1)} %fusion.12) | copy-start | bytes 1572868
  144.7 31.0 %all-to-all-start = ((bf16[4,128,2048]{2,1,0:T(8,128)(2,1)}), bf16[4,128,2048]{2,1,0:T(8,128)(2,1)}, u32[]{:S(2)}, u32[]{:S(2)}) async-start(bf16[4,128,2048]{2,1,0:T(8,128)(2,1)} %broadcast_in_dim.6), calls=%async_computation | async-start | bytes 4194304 | tf_op jit(solution)/shard_map/all_to_all | solution.py:30
  154.5 5.5 %copy-start.1 = (bf16[1,1024,2048]{2,1,0:T(8,128)(2,1)S(1)}, bf16[1,1024,2048]{2,1,0:T(8,128)(2,1)}, u32[]{:S(2)}) copy-start(bf16[1,1024,2048]{2,1,0:T(8,128)(2,1)} %slice_bitcast_fusion) | copy-start | bytes 12582916
  166.1 20.3 %copy-start.7 = (f32[128,2]{0,1:T(2,128)S(1)}, f32[128,2]{0,1:T(2,128)}, u32[]{:S(2)}) copy-start(f32[128,2]{0,1:T(2,128)} %param.23) | copy-start | bytes 3076
  175.7 61.9 %all-to-all-start.2 = ((bf16[64,8,2048]{2,1,0:T(8,128)(2,1)}), bf16[64,8,2048]{2,1,0:T(8,128)(2,1)}, u32[]{:S(2)}, u32[]{:S(2)}) async-start(bf16[64,8,2048]{2,1,0:T(8,128)(2,1)} %fusion.2), calls=%async_computation.2 | async-start | bytes 4194304 | tf_op jit(solution)/shard_map/all_to_all | solution.py:130
Sparse Core Ops, SparseCore 0:
  14.3 124.0 all-gather.1
where the time goes:
time: 257 us
  waiting for transfers between devices  152 us (59%)
  starting transfers between devices  31.1 us (12%)
  local copies, waits for them, and re-layouts  25 us (10%)
  matrix products  17.2 us (7%)
  other arithmetic  16.6 us (6%)
  between operations  14.3 us (6%)
    all_gather x1, waiting for transfers between devices, turned_gather(): whole, at, done = (lax.all_gather(both, axis, axis=0, tiled=True), 0, [])  91.8 us
    all_to_all x1, waiting for transfers between devices, local(): lax.all_to_all(summed.reshape(expert_count, slot_cap, model_width), 'ep',...  47.3 us
    all_to_all x1, starting transfers between devices, local(): lax.all_to_all(outgoing, 'ep', split_axis=0, concat_axis=0, tiled=True)  12.2 us
    all_to_all x1, starting transfers between devices, local(): lax.all_to_all(summed.reshape(expert_count, slot_cap, model_width), 'ep',...  10.7 us
    all_to_all x1, waiting for transfers between devices, sent_to_all(): lax.all_to_all(jnp.broadcast_to(x[None], (count, *x.shape)), axis, 0, 0,...  9.56 us
    reduce_sum x1, other arithmetic, local(): jnp.sum(picked * route_share[:, :, None], axis=1).astype(jnp.bfloat16)  5.59 us
    dot_general x1, matrix products, expert_hidden(): up_proj = jnp.dot(slot_rows, w_up, preferred_element_type=jnp.float32)  5.5 us
    dot_general x1, matrix products, expert_hidden(): gate_proj = jnp.dot(slot_rows, w_gate, preferred_element_type=jnp.float32)  5.18 us
  transfers between devices with their start and end apart: 5, of which 4 were waited for; matrix products, arithmetic and copies ran while one was open for 15% of the time, Pallas kernels for 0%

commit v1 on v0

--- a/solution.py
+++ b/solution.py
@@ -17,7 +17,13 @@
 def turned_gather(arrays, axis, dims):
     turned = [jnp.moveaxis(a, dim, 0) for a, dim in zip(arrays, dims)]
     both = jnp.concatenate([t.reshape(len(t), -1) for t in turned], axis=1)
-    whole, at, done = (lax.all_gather(both, axis, axis=0, tiled=True), 0, [])
+    whole, at, done = (
+        jnp.concatenate(
+            lax.all_to_all(jnp.stack([both] * lax.axis_size(axis)), axis, 0, 0), axis=0
+        ),
+        0,
+        [],
+    )
     for t, dim in zip(turned, dims):
         piece = whole[:, at : at + t[0].size].reshape(-1, *t.shape[1:])
         done.append(jnp.moveaxis(piece, 0, dim))

time: 257 us -> 327 us (1.27)
  waiting for transfers between devices: 152 us -> 226 us
  between operations: 14.3 us -> 0.92 us
  local copies, waits for them, and re-layouts: 25 us -> 32.4 us
    all_to_all x0 -> x1, waiting for transfers between devices: none -> 130 us  [turned_gather(): lax.all_to_all(jnp.stack([both] * lax.axis_size(axis)), axis, 0, 0)]
    all_gather x1 -> x0, waiting for transfers between devices: 91.8 us -> none  [turned_gather(): whole, at, done = (lax.all_gather(both, axis, axis=0, tiled=True), 0, [])]
    all_to_all x1, waiting for transfers between devices: 0.01 us -> 35.4 us  [local(): lax.all_to_all(outgoing, 'ep', split_axis=0, concat_axis=0, tiled=True)]
    another operation x1 -> x2, local copies, waits for them, and re-layouts: 0.01 us -> 7.95 us  [the longest x1 7.94 us: turned_gather(): jnp.stack([both] * lax.axis_size(axis))]
    all_to_all x0 -> x1, starting transfers between devices: none -> 6.46 us  [turned_gather(): lax.all_to_all(jnp.stack([both] * lax.axis_size(axis)), axis, 0, 0)]
  transfers between devices with their start and end apart: 5 -> 5, of which waited for: 4 -> 5; matrix products, arithmetic and copies ran while one was open for 15% -> 11% of each run, Pallas kernels for 0% -> 0%
where the time goes in v1:
time: 327 us
  waiting for transfers between devices  226 us (69%)
  starting transfers between devices  33.4 us (10%)
  local copies, waits for them, and re-layouts  32.4 us (10%)
  matrix products  17.2 us (5%)
  other arithmetic  16.5 us (5%)
    all_to_all x1, waiting for transfers between devices, turned_gather(): lax.all_to_all(jnp.stack([both] * lax.axis_size(axis)), axis, 0, 0)  130 us
    all_to_all x1, waiting for transfers between devices, local(): lax.all_to_all(summed.reshape(expert_count, slot_cap, model_width), 'ep',...  47.3 us
    all_to_all x1, waiting for transfers between devices, local(): lax.all_to_all(outgoing, 'ep', split_axis=0, concat_axis=0, tiled=True)  35.4 us
    all_to_all x1, starting transfers between devices, local(): lax.all_to_all(outgoing, 'ep', split_axis=0, concat_axis=0, tiled=True)  12.2 us
    all_to_all x1, waiting for transfers between devices, sent_to_all(): lax.all_to_all(jnp.broadcast_to(x[None], (count, *x.shape)), axis, 0, 0,...  8.19 us
    another operation x1, local copies, waits for them, and re-layouts, turned_gather(): jnp.stack([both] * lax.axis_size(axis))  7.94 us
    all_to_all x1, starting transfers between devices, local(): lax.all_to_all(summed.reshape(expert_count, slot_cap, model_width), 'ep',...  7.58 us
  transfers between devices with their start and end apart: 5, of which 5 were waited for; matrix products, arithmetic and copies ran while one was open for 11% of the time, Pallas kernels for 0%

profile of v1, /device:TPU:2, one launch (start us, length us, event | category | flops | bytes accessed | tf_op | source)
XLA Modules:
  0.0 326.5 jit_solution(2211187910795424601)
XLA Ops:
  0.6 0.0 copy-start
  0.6 1.6 copy.31
  2.3 2.3 copy.30
  4.6 3.0 pad_maximum_fusion
  7.6 7.9 %stack.2 = bf16[4,256,6144]{2,1,0:T(8,128)(2,1)} broadcast(bf16[256,6144]{1,0:T(8,128)(2,1)} %pad_maximum_fusion), dimensions={1,2} | broadcast | bytes 15728640 | tf_op jit(solution)/shard_map/stack | solution.py:22
  15.5 6.5 %all-to-all-start.2 = ((bf16[4,256,6144]{2,1,0:T(8,128)(2,1)}), bf16[4,256,6144]{2,1,0:T(8,128)(2,1)}, u32[]{:S(2)}, u32[]{:S(2)}) async-start(bf16[4,256,6144]{2,1,0:T(8,128)(2,1)} %stack.2), calls=%async_computation.2 | async-start | bytes 25165824 | tf_op jit(solution)/shard_map/all_to_all | solution.py:22
  22.0 0.1 copy.25
  22.1 0.1 eq.38
  22.3 0.1 eq.42
  22.4 0.6 reduce-window.6
  23.0 0.2 slice_reduce_fusion
  23.3 0.1 fusion.25
  23.4 0.1 reshape.109
  23.5 0.1 copy.28
  23.6 0.1 copy.29
  23.7 0.1 reshape.110
  23.9 0.2 fusion.13
  24.1 0.2 fusion.15
  24.3 0.6 broadcast_in_dim.8
  24.9 1.2 reshape.134
  26.2 4.5 %scatter_custom_fusion = bf16[512,2048]{1,0:T(8,128)(2,1)} fusion(s32[256]{0:T(256)S(1)} %bitcast.82, bf16[256,2048]{1,0:T(8,128)(2,1)} %reshape.134, bf16[]{:T(256)} %constant.45.clone.1), kind=kCustom, calls=%fused_computation.38 | custom fusion | bytes 2097664 | tf_op jit(solution)/shard_map/scatter | solution.py:63
  30.6 130.4 %all-to-all-done.2 = bf16[4,256,6144]{2,1,0:T(8,128)(2,1)} async-done(((bf16[4,256,6144]{2,1,0:T(8,128)(2,1)}), bf16[4,256,6144]{2,1,0:T(8,128)(2,1)}, u32[]{:S(2)}, u32[]{:S(2)}) %all-to-all-start.2) | async-done | bytes 12582944 | tf_op jit(solution)/shard_map/all_to_all | solution.py:22
  161.0 12.2 %all-to-all-start.1 = ((bf16[64,8,2048]{2,1,0:T(8,128)(2,1)}), bf16[64,8,2048]{2,1,0:T(8,128)(2,1)}, u32[]{:S(2)}, u32[]{:S(2)}) async-start(bf16[64,8,2048]{2,1,0:T(8,128)(2,1)} %bitcast.75), calls=%async_computation.1 | async-start | bytes 4194304 | tf_op jit(solution)/shard_map/all_to_all | solution.py:123
  173.2 0.0 copy-start.4
  173.2 1.3 convert_multiply_fusion.2
  174.6 2.5 collective-permute-start
  177.2 4.8 %collective-permute-done = f32[2,2048]{1,0:T(2,128)S(1)} collective-permute-done((f32[2,2048]{1,0:T(2,128)S(1)}, f32[2,2048]{1,0:T(2,128)S(1)}, u32[]{:S(2)}, u32[]{:S(2)}) %collective-permute-start) | collective-permute-done | bytes 16416 | tf_op jit(solution)/shard_map/ppermute | solution.py:14
  182.0 2.2 fusion.12
  184.2 4.8 %slice_bitcast_fusion = bf16[1,1024,2048]{2,1,0:T(8,128)(2,1)} fusion(bf16[1024,6144]{1,0:T(8,128)(2,1)} %bitcast.13), kind=kLoop, calls=%fused_computation.2 | loop fusion | bytes 8388608 | tf_op jit(solution)/shard_map/transpose;reshape | solution.py:29
  189.0 35.4 %all-to-all-done.1 = bf16[64,8,2048]{2,1,0:T(8,128)(2,1)} async-done(((bf16[64,8,2048]{2,1,0:T(8,128)(2,1)}), bf16[64,8,2048]{2,1,0:T(8,128)(2,1)}, u32[]{:S(2)}, u32[]{:S(2)}) %all-to-all-start.1) | async-done | bytes 2097184 | tf_op jit(solution)/shard_map/all_to_all | solution.py:123
  224.4 0.0 copy-done.3
  224.4 1.6 broadcast_in_dim.6
  226.0 4.6 %all-to-all-start = ((bf16[4,128,2048]{2,1,0:T(8,128)(2,1)}), bf16[4,128,2048]{2,1,0:T(8,128)(2,1)}, u32[]{:S(2)}, u32[]{:S(2)}) async-start(bf16[4,128,2048]{2,1,0:T(8,128)(2,1)} %broadcast_in_dim.6), calls=%async_computation | async-start | bytes 4194304 | tf_op jit(solution)/shard_map/all_to_all | solution.py:36
  230.6 5.2 %fusion.1 = f32[512,1024]{1,0:T(8,128)S(1)} fusion(bf16[1024,6144]{1,0:T(8,128)(2,1)} %bitcast.13, bf16[64,8,2048]{2,1,0:T(8,128)(2,1)} %all-to-all-done.1), kind=kOutput, calls=%fused_computation.6 | convolution fusion | flops 2147483648 | bytes 8388608 | tf_op jit(solution)/shard_map/dot_general | solution.py:67
  235.8 5.5 %multiply_convert_fusion = bf16[512,1024]{1,0:T(8,128)(2,1)S(1)} fusion(f32[512,1024]{1,0:T(8,128)S(1)} %fusion.1, bf16[1024,6144]{1,0:T(8,128)(2,1)} %bitcast.13, bf16[64,8,2048]{2,1,0:T(8,128)(2,1)} %all-to-all-done.1), kind=kOutput, calls=%fused_computation.17 | convolution fusion | flops 2150629376 | bytes 9437184 | tf_op jit(solution)/shard_map/dot_general | solution.py:68
  241.3 0.7 convolution_convert_fusion
  242.1 0.7 convolution_convert_fusion.1
  242.8 0.7 convolution_convert_fusion.2
  243.5 0.7 convolution_convert_fusion.3
  244.2 3.1 fusion.2
  247.4 8.2 %all-to-all-done = bf16[4,128,2048]{2,1,0:T(8,128)(2,1)} async-done(((bf16[4,128,2048]{2,1,0:T(8,128)(2,1)}), bf16[4,128,2048]{2,1,0:T(8,128)(2,1)}, u32[]{:S(2)}, u32[]{:S(2)}) %all-to-all-start) | async-done | bytes 2097184 | tf_op jit(solution)/shard_map/all_to_all | solution.py:36
  255.6 7.6 %all-to-all-start.3 = ((bf16[64,8,2048]{2,1,0:T(8,128)(2,1)}), bf16[64,8,2048]{2,1,0:T(8,128)(2,1)}, u32[]{:S(2)}, u32[]{:S(2)}) async-start(bf16[64,8,2048]{2,1,0:T(8,128)(2,1)} %fusion.2), calls=%async_computation.3 | async-start | bytes 4194304 | tf_op jit(solution)/shard_map/all_to_all | solution.py:136
  263.2 0.1 copy.32
  263.4 3.6 %convolution_convert_fusion.4 = bf16[512,512]{1,0:T(8,128)(2,1)} fusion(bf16[512,2048]{1,0:T(8,128)(2,1)} %bitcast.3, bf16[2048,512]{1,0:T(8,128)(2,1)S(1)} %copy-done), kind=kOutput, calls=%fused_computation.20 | convolution fusion | flops 1074003968 | bytes 4718592 | tf_op jit(solution)/shard_map/dot_general | solution.py:117
  267.0 47.3 %all-to-all-done.3 = bf16[64,8,2048]{2,1,0:T(8,128)(2,1)} async-done(((bf16[64,8,2048]{2,1,0:T(8,128)(2,1)}), bf16[64,8,2048]{2,1,0:T(8,128)(2,1)}, u32[]{:S(2)}, u32[]{:S(2)}) %all-to-all-start.3) | async-done | bytes 2097184 | tf_op jit(solution)/shard_map/all_to_all | solution.py:136
  314.3 4.2 %gather_fusion = bf16[256,2048]{1,0:T(8,128)(2,1)S(1)} fusion(bf16[512,2048]{1,0:T(8,128)(2,1)} %bitcast.26, s32[1024]{0:T(1024)S(1)} %pad_clamp_fusion), kind=kCustom, calls=%fused_computation | custom fusion | bytes 2098176 | tf_op jit(solution)/shard_map/gather | solution.py:143
  318.5 2.4 reshape.121
  320.9 5.6 %multiply_reduce_fusion = bf16[128,2048]{1,0:T(8,128)(2,1)} fusion(f32[128,2,2048]{2,1,0:T(2,128)} %reshape.121, f32[128,2]{1,0:T(8,128)S(1)} %copy.32), kind=kLoop, calls=%fused_computation.16 | loop fusion | flops 786432 | bytes 2622464 | tf_op jit(solution)/shard_map/reduce_sum | solution.py:147
  (25 shorter events, 0.2 us)
Async XLA Ops:
  0.6 262.7 %copy-start = (bf16[2048,512]{1,0:T(8,128)(2,1)S(1)}, bf16[2048,512]{1,0:T(8,128)(2,1)}, u32[]{:S(2)}) copy-start(bf16[2048,512]{1,0:T(8,128)(2,1)} %param.16) | copy-start | bytes 6291460
  15.5 6.5 %copy-start.6 = (s32[128,2]{0,1:T(2,128)S(1)}, s32[128,2]{0,1:T(2,128)}, u32[]{:S(2)}) copy-start(s32[128,2]{0,1:T(2,128)} %param.22) | copy-start | bytes 3076
  15.5 8.3 %copy-start.2 = (bf16[128,2048]{1,0:T(8,128)(2,1)S(1)}, bf16[128,2048]{1,0:T(8,128)(2,1)}, u32[]{:S(2)}) copy-start(bf16[128,2048]{1,0:T(8,128)(2,1)} %param.17) | copy-start | bytes 1572868
  15.5 8.6 %copy-start.5 = (f32[2048]{0:T(1024)S(1)}, f32[2048]{0:T(1024)}, u32[]{:S(2)}) copy-start(f32[2048]{0:T(1024)} %param.18) | copy-start | bytes 24580
  15.5 145.5 %all-to-all-start.2 = ((bf16[4,256,6144]{2,1,0:T(8,128)(2,1)}), bf16[4,256,6144]{2,1,0:T(8,128)(2,1)}, u32[]{:S(2)}, u32[]{:S(2)}) async-start(bf16[4,256,6144]{2,1,0:T(8,128)(2,1)} %stack.2), calls=%async_computation.2 | async-start | bytes 25165824 | tf_op jit(solution)/shard_map/all_to_all | solution.py:22
  161.0 63.4 %all-to-all-start.1 = ((bf16[64,8,2048]{2,1,0:T(8,128)(2,1)}), bf16[64,8,2048]{2,1,0:T(8,128)(2,1)}, u32[]{:S(2)}, u32[]{:S(2)}) async-start(bf16[64,8,2048]{2,1,0:T(8,128)(2,1)} %bitcast.75), calls=%async_computation.1 | async-start | bytes 4194304 | tf_op jit(solution)/shard_map/all_to_all | solution.py:123
  173.2 3.9 %copy-start.4 = (bf16[3,2048]{1,0:T(4,128)(2,1)S(1)}, bf16[3,2048]{1,0:T(4,128)(2,1)}, u32[]{:S(2)}) copy-start(bf16[3,2048]{1,0:T(4,128)(2,1)} %param.15) | copy-start | bytes 36868
  174.6 7.4 %collective-permute-start = (f32[2,2048]{1,0:T(2,128)S(1)}, f32[2,2048]{1,0:T(2,128)S(1)}, u32[]{:S(2)}, u32[]{:S(2)}) collective-permute-start(f32[2,2048]{1,0:T(2,128)S(1)} %slice.78), channel_id=1, source_target_pairs={{0,1},{1,2},{2,3},{3,4},{4,5},{5,6},{6,7},{7,8},{8,9},{9,10},{10,1... | collective-permute-start | bytes 49160 | tf_op jit(solution)/shard_map/ppermute | solution.py:14
  184.2 40.2 %copy-start.3 = (bf16[128,2048]{1,0:T(8,128)(2,1)S(1)}, bf16[128,2048]{1,0:T(8,128)(2,1)}, u32[]{:S(2)}) copy-start(bf16[128,2048]{1,0:T(8,128)(2,1)} %fusion.12) | copy-start | bytes 1572868
  226.0 29.6 %all-to-all-start = ((bf16[4,128,2048]{2,1,0:T(8,128)(2,1)}), bf16[4,128,2048]{2,1,0:T(8,128)(2,1)}, u32[]{:S(2)}, u32[]{:S(2)}) async-start(bf16[4,128,2048]{2,1,0:T(8,128)(2,1)} %broadcast_in_dim.6), calls=%async_computation | async-start | bytes 4194304 | tf_op jit(solution)/shard_map/all_to_all | solution.py:36
  235.8 5.5 %copy-start.1 = (bf16[1,1024,2048]{2,1,0:T(8,128)(2,1)S(1)}, bf16[1,1024,2048]{2,1,0:T(8,128)(2,1)}, u32[]{:S(2)}) copy-start(bf16[1,1024,2048]{2,1,0:T(8,128)(2,1)} %slice_bitcast_fusion) | copy-start | bytes 12582916
  247.4 15.8 %copy-start.7 = (f32[128,2]{0,1:T(2,128)S(1)}, f32[128,2]{0,1:T(2,128)}, u32[]{:S(2)}) copy-start(f32[128,2]{0,1:T(2,128)} %param.23) | copy-start | bytes 3076
  255.6 58.7 %all-to-all-start.3 = ((bf16[64,8,2048]{2,1,0:T(8,128)(2,1)}), bf16[64,8,2048]{2,1,0:T(8,128)(2,1)}, u32[]{:S(2)}, u32[]{:S(2)}) async-start(bf16[64,8,2048]{2,1,0:T(8,128)(2,1)} %fusion.2), calls=%async_computation.3 | async-start | bytes 4194304 | tf_op jit(solution)/shard_map/all_to_all | solution.py:136
